TPU v7x, 512 devices: a whole 4x8x8 slice. The times are simulated.
512 devices in a mesh: ep: 128 (over z, y, core), tp: 4 (over x).
Axes of the slice: x: 4, y: 8, z: 8, core: 2. Of those that a mesh axis runs over, the one named last changes fastest.
Arguments:
- tokens: bfloat16 [16384, 2048], P('ep'), may hold values from -6 to 6
- norm_gain: float32 [2048], replicated, may hold values from 0.1 to 1.9
- routes: int32 [16384, 2], P('ep'), may hold values from 0 to 127, all different within a row; in each aligned block of 128 rows (0 to 127, 128 to 255, ...) at most 3 rows name the same one
- group_prob: float32 [16384], P('ep'), may hold values from 0.2 to 1
- expert_logits: float32 [16384, 2], P('ep'), may hold values from -6 to 6
- gate_weight: bfloat16 [128, 2048, 384], P('ep', None, 'tp'), may hold values from -0.125 to 0.125
- up_weight: bfloat16 [128, 2048, 384], P('ep', None, 'tp'), may hold values from -0.125 to 0.125
- down_matrix: bfloat16 [128, 384, 2048], P('ep', 'tp'), may hold values from -0.3125 to 0.3125
Outputs:
- combined: bfloat16 [16384, 2048], P('ep', 'tp')
Inputs may be any that keep to these rules, and one draw needn't show every extreme that they name: `routes`: each row names 2 different experts. Among the 128 tokens of one index of ep at most 3 rows name one expert, and in every draw some expert is named by exactly 3 of them.
All inputs are finite; a program needn't handle non-finite values.
Results may differ from a plain program's by a relative error of at most 0.013.
Values may be sent and summed in bfloat16 or wider, within the bound.
A program may use at most 64 MiB of HBM per device.

v0:
```python
import jax
import jax.numpy as jnp
from jax import lax
from jax.sharding import PartitionSpec as P


def in_order(parts, dim):
    lengths = list(parts.shape[1:])
    lengths[dim] *= parts.shape[0]
    return jnp.moveaxis(parts, 0, dim).reshape(lengths)


def sent_to_all(shard, axis):
    copies = jnp.broadcast_to(shard, (lax.axis_size(axis), *shard.shape))
    return lax.all_to_all(copies, axis, split_axis=0, concat_axis=0, tiled=True)


def gathered_copies(shard, axis, dim):
    return in_order(sent_to_all(shard, axis), dim)


def hidden_part(buffer, gate_weight, up_weight):
    local_count = gate_weight.shape[0]
    grouped = buffer.reshape(
        buffer.shape[0] // local_count, local_count, buffer.shape[1], buffer.shape[2]
    )
    gate_proj = jnp.einsum(
        "sknd,kdf->sknf", grouped, gate_weight, preferred_element_type=jnp.float32
    )
    up_proj = jnp.einsum("sknd,kdf->sknf", grouped, up_weight, preferred_element_type=jnp.float32)
    hidden_state = (jax.nn.silu(gate_proj) * up_proj).astype(jnp.bfloat16)
    return hidden_state.reshape(buffer.shape[0], buffer.shape[1], hidden_state.shape[3])


def down_blocks(hidden_full, down_cols, block_count):
    local_count = down_cols.shape[0]
    width = hidden_full.shape[2] // block_count
    grouped = hidden_full.reshape(
        hidden_full.shape[0] // local_count, local_count, hidden_full.shape[1], block_count, width
    )
    columns = down_cols.reshape(local_count, block_count, width, down_cols.shape[2])
    block_list = jnp.einsum(
        "sknrf,krfd->sknrd", grouped, columns, preferred_element_type=jnp.float32
    ).astype(jnp.bfloat16)
    summed = jnp.sum(block_list.astype(jnp.float32), 3).astype(jnp.bfloat16)
    return summed.reshape(hidden_full.shape[0], hidden_full.shape[1], down_cols.shape[2])


def body(tokens, norm_gain, routes, group_prob, expert_logits, gate_weight, up_weight, down_matrix):
    tok_rows, model_width = tokens.shape
    top_count = routes.shape[1]
    experts = gate_weight.shape[0] * lax.axis_size("ep")
    capacity = 3 * top_count * tok_rows // (2 * experts)
    block_count = lax.axis_size("tp")
    down_cols = lax.all_to_all(down_matrix, "tp", split_axis=2, concat_axis=1, tiled=True)
    values = tokens.astype(jnp.float32)
    normed = (
        values * lax.rsqrt(jnp.mean(values * values, -1, keepdims=True) + 1e-06) * norm_gain
    ).astype(jnp.bfloat16)
    flat_ids = routes.reshape(-1)
    onehot = (flat_ids[:, None] == jnp.arange(experts, dtype=jnp.int32)[None, :]).astype(jnp.int32)
    earlier = jnp.cumsum(onehot, 0) - onehot
    slot_index = jnp.sum(earlier * onehot, 1)
    target = flat_ids * capacity + slot_index
    owners = jnp.arange(tok_rows * top_count, dtype=jnp.int32) // top_count
    outgoing = (
        jnp.zeros((experts * capacity, model_width), jnp.bfloat16).at[target].set(normed[owners])
    )
    outgoing = outgoing.reshape(experts, capacity, model_width)
    feature_share = model_width // block_count
    my_features = lax.dynamic_slice_in_dim(
        outgoing, lax.axis_index("tp") * feature_share, feature_share, 2
    )
    arrived = lax.all_to_all(my_features, "ep", split_axis=0, concat_axis=0, tiled=True)
    full_rows = gathered_copies(arrived, "tp", 2)
    hidden_state = hidden_part(full_rows, gate_weight, up_weight)
    hidden_full = gathered_copies(hidden_state, "tp", 2)
    summed = down_blocks(hidden_full, down_cols, block_count)
    returned = lax.all_to_all(summed, "ep", split_axis=0, concat_axis=0, tiled=True)
    flat_back = returned.reshape(experts * capacity, returned.shape[2])
    weights = group_prob[:, None] * jax.nn.softmax(expert_logits, axis=-1)
    picked = flat_back[target].reshape(tok_rows, top_count, flat_back.shape[1]).astype(jnp.float32)
    combined = jnp.sum(picked * weights[:, :, None], 1).astype(jnp.bfloat16)
    return combined


def solution(mesh):
    return jax.shard_map(
        body,
        mesh=mesh,
        in_specs=(
            P("ep", None),
            P(),
            P("ep", None),
            P("ep"),
            P("ep", None),
            P("ep", None, "tp"),
            P("ep", None, "tp"),
            P("ep", "tp", None),
        ),
        out_specs=P("ep", "tp"),
        check_vma=False,
    )
```

profile of v0, /device:TPU:1, one launch (start us, length us, event | category | flops | bytes accessed | tf_op | source)
XLA Modules:
  0.0 136.8 jit_solution(1834693873175598776)
XLA Ops:
  0.0 0.9 copy.34
  2.5 1.2 fusion.4
  4.2 5.9 %scatter_custom_fusion = bf16[384,2048]{1,0:T(8,128)(2,1)S(1)} fusion(s32[256]{0:T(256)S(1)} %bitcast.72, bf16[128,2048]{1,0:T(8,128)(2,1)S(1)} %fusion.6, s32[1024]{0:T(1024)S(1)} %pad_clamp_fusion.1, bf16[]{:T(256)} %constant.18.clone.1), kind=kCustom, calls=%fused_computation.15 | custom fusion | bytes 1572866 | tf_op jit(solution)/shard_map/scatter | solution.py:67
  10.1 2.3 %reshape.142 = bf16[128,3,2048]{2,1,0:T(4,128)(2,1)} reshape(bf16[384,2048]{1,0:T(8,128)(2,1)S(1)} %scatter_custom_fusion) | data formatting | bytes 3145728 | tf_op jit(solution)/shard_map/reshape | solution.py:69
  12.5 2.1 %constant_dynamic-slice_fusion = bf16[128,3,512]{2,1,0:T(4,128)(2,1)} fusion(bf16[128,3,2048]{2,1,0:T(4,128)(2,1)} %reshape.142, s32[]{:T(128)S(6)} %select_n.39), kind=kLoop, calls=%fused_computation.46 | loop fusion | bytes 786436 | tf_op jit(solution)/shard_map/dynamic_slice | solution.py:71
  14.5 18.4 %all-to-all-start.1 = ((bf16[128,3,512]{2,1,0:T(4,128)(2,1)}), bf16[128,3,512]{2,1,0:T(4,128)(2,1)S(1)}, u32[]{:S(2)}, u32[]{:S(2)}) async-start(bf16[128,3,512]{2,1,0:T(4,128)(2,1)} %constant_dynamic-slice_fusion), calls=%async_computation.1 | async-start | bytes 1048576 | tf_op jit(solution)/shard_map/all_to_all | solution.py:74
  33.0 0.8 copy.28
  34.2 11.5 %reduce.4 = bf16[2048,96]{1,0:T(8,128)(2,1)S(1)} reduce(bf16[2048,1,96]{2,1,0:T(2,128)(2,1)S(1)} %bitcast.65, bf16[]{:T(256)} %broadcast.137), dimensions={1}, to_apply=%bitcast.53.reduce_sub_computation | reduce | bytes 786434
  45.8 1.6 %reshape.182 = bf16[4,2,24576]{2,1,0:T(2,128)(2,1)} reshape(bf16[2048,96]{1,0:T(8,128)(2,1)S(1)} %reduce.4) | data formatting | bytes 786432
  47.3 6.2 %all-to-all-done.1 = bf16[128,3,512]{2,1,0:T(4,128)(2,1)S(1)} async-done(((bf16[128,3,512]{2,1,0:T(4,128)(2,1)}), bf16[128,3,512]{2,1,0:T(4,128)(2,1)S(1)}, u32[]{:S(2)}, u32[]{:S(2)}) %all-to-all-start.1) | async-done | bytes 393248 | tf_op jit(solution)/shard_map/all_to_all | solution.py:74
  53.5 4.0 %all-to-all-start = ((bf16[4,2,24576]{2,1,0:T(2,128)(2,1)}), bf16[4,2,24576]{2,1,0:T(2,128)(2,1)S(1)}, u32[]{:S(2)}, u32[]{:S(2)}) async-start(bf16[4,2,24576]{2,1,0:T(2,128)(2,1)} %reshape.182), calls=%async_computation | async-start | bytes 786432 | tf_op jit(solution)/shard_map/all_to_all | solution.py:55
  57.6 8.1 %all-to-all-done = bf16[4,2,24576]{2,1,0:T(2,128)(2,1)S(1)} async-done(((bf16[4,2,24576]{2,1,0:T(2,128)(2,1)}), bf16[4,2,24576]{2,1,0:T(2,128)(2,1)S(1)}, u32[]{:S(2)}, u32[]{:S(2)}) %all-to-all-start) | async-done | bytes 393248 | tf_op jit(solution)/shard_map/all_to_all | solution.py:55
  65.7 1.3 broadcast_in_dim.7
  67.0 3.6 %all-to-all-start.2 = ((bf16[4,128,3,512]{3,1,2,0:T(8,128)(2,1)}), bf16[4,128,3,512]{3,1,2,0:T(8,128)(2,1)S(1)}, u32[]{:S(2)}, u32[]{:S(2)}) async-start(bf16[4,128,3,512]{3,1,2,0:T(8,128)(2,1)} %broadcast_in_dim.7), calls=%async_computation.2 | async-start | bytes 3145728 | tf_op jit(solution)/shard_map/all_to_all | solution.py:15
  70.5 0.8 reshape.183
  71.3 19.1 %all-to-all-done.2 = bf16[4,128,3,512]{3,1,2,0:T(8,128)(2,1)S(1)} async-done(((bf16[4,128,3,512]{3,1,2,0:T(8,128)(2,1)}), bf16[4,128,3,512]{3,1,2,0:T(8,128)(2,1)S(1)}, u32[]{:S(2)}, u32[]{:S(2)}) %all-to-all-start.2) | async-done | bytes 1572896 | tf_op jit(solution)/shard_map/all_to_all | solution.py:15
  93.0 3.5 %all-to-all-start.3 = ((bf16[4,128,3,96]{1,3,2,0:T(8,128)(2,1)}), bf16[4,128,3,96]{1,3,2,0:T(8,128)(2,1)S(1)}, u32[]{:S(2)}, u32[]{:S(2)}) async-start(bf16[4,128,3,96]{1,3,2,0:T(8,128)(2,1)} %broadcast_in_dim.8), calls=%async_computation.3 | async-start | bytes 589824 | tf_op jit(solution)/shard_map/all_to_all | solution.py:15
  96.4 1.1 fusion.19
  98.1 4.0 %all-to-all-done.3 = bf16[4,128,3,96]{1,3,2,0:T(8,128)(2,1)S(1)} async-done(((bf16[4,128,3,96]{1,3,2,0:T(8,128)(2,1)}), bf16[4,128,3,96]{1,3,2,0:T(8,128)(2,1)S(1)}, u32[]{:S(2)}, u32[]{:S(2)}) %all-to-all-start.3) | async-done | bytes 294944 | tf_op jit(solution)/shard_map/all_to_all | solution.py:15
  102.7 1.2 copy.40
  103.9 9.1 %all-to-all-start.4 = ((bf16[128,3,512]{2,1,0:T(4,128)(2,1)}), bf16[128,3,512]{2,1,0:T(4,128)(2,1)S(1)}, u32[]{:S(2)}, u32[]{:S(2)}) async-start(bf16[128,3,512]{2,1,0:T(4,128)(2,1)} %copy.40), calls=%async_computation.4 | async-start | bytes 1048576 | tf_op jit(solution)/shard_map/all_to_all | solution.py:79
  113.2 20.4 %all-to-all-done.4 = bf16[128,3,512]{2,1,0:T(4,128)(2,1)S(1)} async-done(((bf16[128,3,512]{2,1,0:T(4,128)(2,1)}), bf16[128,3,512]{2,1,0:T(4,128)(2,1)S(1)}, u32[]{:S(2)}, u32[]{:S(2)}) %all-to-all-start.4) | async-done | bytes 393248 | tf_op jit(solution)/shard_map/all_to_all | solution.py:79
  133.9 1.2 gather_fusion
  135.4 1.4 multiply_reduce_fusion
  (52 shorter events, 7.1 us)
Async XLA Ops:
  0.0 90.6 %copy-start = (bf16[1,2048,96]{1,2,0:T(8,128)(2,1)S(1)}, bf16[1,2048,96]{1,2,0:T(8,128)(2,1)}, u32[]{:S(2)}) copy-start(bf16[1,2048,96]{1,2,0:T(8,128)(2,1)} %param.13) | copy-start | bytes 1179652
  0.0 4.0 %copy-start.1 = (bf16[128,2048]{1,0:T(8,128)(2,1)S(1)}, bf16[128,2048]{1,0:T(8,128)(2,1)}, u32[]{:S(2)}) copy-start(bf16[128,2048]{1,0:T(8,128)(2,1)} %param.8) | copy-start | bytes 1572868
  0.0 4.0 %copy-start.4 = (f32[2048]{0:T(1024)S(1)}, f32[2048]{0:T(1024)}, u32[]{:S(2)}) copy-start(f32[2048]{0:T(1024)} %param.9) | copy-start | bytes 24580
  12.5 20.5 %copy-start.2 = (bf16[1,96,2048]{2,1,0:T(8,128)(2,1)S(1)}, bf16[1,96,2048]{2,1,0:T(8,128)(2,1)}, u32[]{:S(2)}) copy-start(bf16[1,96,2048]{2,1,0:T(8,128)(2,1)} %param.15) | copy-start | bytes 1179652
  14.5 39.0 %all-to-all-start.1 = ((bf16[128,3,512]{2,1,0:T(4,128)(2,1)}), bf16[128,3,512]{2,1,0:T(4,128)(2,1)S(1)}, u32[]{:S(2)}, u32[]{:S(2)}) async-start(bf16[128,3,512]{2,1,0:T(4,128)(2,1)} %constant_dynamic-slice_fusion), calls=%async_computation.1 | async-start | bytes 1048576 | tf_op jit(solution)/shard_map/all_to_all | solution.py:74
  53.5 12.2 %all-to-all-start = ((bf16[4,2,24576]{2,1,0:T(2,128)(2,1)}), bf16[4,2,24576]{2,1,0:T(2,128)(2,1)S(1)}, u32[]{:S(2)}, u32[]{:S(2)}) async-start(bf16[4,2,24576]{2,1,0:T(2,128)(2,1)} %reshape.182), calls=%async_computation | async-start | bytes 786432 | tf_op jit(solution)/shard_map/all_to_all | solution.py:55
  67.0 23.5 %all-to-all-start.2 = ((bf16[4,128,3,512]{3,1,2,0:T(8,128)(2,1)}), bf16[4,128,3,512]{3,1,2,0:T(8,128)(2,1)S(1)}, u32[]{:S(2)}, u32[]{:S(2)}) async-start(bf16[4,128,3,512]{3,1,2,0:T(8,128)(2,1)} %broadcast_in_dim.7), calls=%async_computation.2 | async-start | bytes 3145728 | tf_op jit(solution)/shard_map/all_to_all | solution.py:15
  90.6 1.0 copy-start.6
  93.0 9.1 %all-to-all-start.3 = ((bf16[4,128,3,96]{1,3,2,0:T(8,128)(2,1)}), bf16[4,128,3,96]{1,3,2,0:T(8,128)(2,1)S(1)}, u32[]{:S(2)}, u32[]{:S(2)}) async-start(bf16[4,128,3,96]{1,3,2,0:T(8,128)(2,1)} %broadcast_in_dim.8), calls=%async_computation.3 | async-start | bytes 589824 | tf_op jit(solution)/shard_map/all_to_all | solution.py:15
  102.1 11.0 %copy-start.3 = (f32[128,2]{0,1:T(2,128)S(1)}, f32[128,2]{0,1:T(2,128)}, u32[]{:S(2)}) copy-start(f32[128,2]{0,1:T(2,128)} %param.12) | copy-start | bytes 3076
  102.1 11.0 %copy-start.5 = (f32[128]{0:T(128)S(1)}, f32[128]{0:T(128)}, u32[]{:S(2)}) copy-start(f32[128]{0:T(128)} %param.11) | copy-start | bytes 1540
  103.9 29.7 %all-to-all-start.4 = ((bf16[128,3,512]{2,1,0:T(4,128)(2,1)}), bf16[128,3,512]{2,1,0:T(4,128)(2,1)S(1)}, u32[]{:S(2)}, u32[]{:S(2)}) async-start(bf16[128,3,512]{2,1,0:T(4,128)(2,1)} %copy.40), calls=%async_computation.4 | async-start | bytes 1048576 | tf_op jit(solution)/shard_map/all_to_all | solution.py:79
where the time goes:
time: 137 us
  waiting for transfers between devices  57.7 us (42%)
  starting transfers between devices  38.6 us (28%)
  local copies, waits for them, and re-layouts  22.9 us (17%)
  other arithmetic  15.6 us (11%)
  matrix products  1.82 us (1%)
    all_to_all x2, waiting for transfers between devices, sent_to_all(): return lax.all_to_all(copies, axis, split_axis=0, concat_axis=0, tiled=True)  23.1 us
    all_to_all x1, waiting for transfers between devices, body(): lax.all_to_all(summed, 'ep', split_axis=0, concat_axis=0, tiled=True)  20.4 us
    all_to_all x1, starting transfers between devices, body(): lax.all_to_all(my_features, 'ep', split_axis=0, concat_axis=0, tiled=True)  18.4 us
    unnamed x1, other arithmetic  11.5 us
    all_to_all x1, starting transfers between devices, body(): lax.all_to_all(summed, 'ep', split_axis=0, concat_axis=0, tiled=True)  9.14 us
    all_to_all x1, waiting for transfers between devices, body(): lax.all_to_all(down_matrix, 'tp', split_axis=2, concat_axis=1, tiled=True)  8.05 us
    all_to_all x2, starting transfers between devices, sent_to_all(): return lax.all_to_all(copies, axis, split_axis=0, concat_axis=0, tiled=True)  7.01 us
    all_to_all x1, waiting for transfers between devices, body(): lax.all_to_all(my_features, 'ep', split_axis=0, concat_axis=0, tiled=True)  6.16 us
  transfers between devices with their start and end apart: 5, of which 5 were waited for; matrix products, arithmetic and copies ran while one was open for 12% of the time, Pallas kernels for 0%

commit v1 on v0

--- a/solution.py
+++ b/solution.py
@@ -2,6 +2,29 @@
 import jax.numpy as jnp
 from jax import lax
 from jax.sharding import PartitionSpec as P
+
+
+def in_blocks(x, dim, length):
+    shape = x.shape
+    tiles = x.reshape(*shape[:dim], length, shape[dim] // length, *shape[dim + 1 :])
+    return jnp.moveaxis(tiles, dim, 0)
+
+
+def in_order_2(blocks, dim):
+    shape = list(blocks.shape[1:])
+    shape[dim] *= blocks.shape[0]
+    return jnp.moveaxis(blocks, 0, dim).reshape(shape)
+
+
+def rotated_exchange(x, axis, split_dim, concat_dim):
+    peers, index = (lax.axis_size(axis), lax.axis_index(axis))
+    blocks = in_blocks(x, split_dim, peers)
+    outs = [blocks[index]]
+    for step in range(1, peers):
+        sent = blocks[(index + step) % peers]
+        outs.append(lax.ppermute(sent, axis, [(i, (i + step) % peers) for i in range(peers)]))
+    blocks = jnp.stack(outs)[(index - jnp.arange(peers)) % peers]
+    return in_order_2(blocks, concat_dim)
 
 
 def in_order(parts, dim):
@@ -52,7 +75,7 @@
     experts = gate_weight.shape[0] * lax.axis_size("ep")
     capacity = 3 * top_count * tok_rows // (2 * experts)
     block_count = lax.axis_size("tp")
-    down_cols = lax.all_to_all(down_matrix, "tp", split_axis=2, concat_axis=1, tiled=True)
+    down_cols = rotated_exchange(down_matrix, "tp", 2, 1)
     values = tokens.astype(jnp.float32)
     normed = (
         values * lax.rsqrt(jnp.mean(values * values, -1, keepdims=True) + 1e-06) * norm_gain

time: 137 us -> 124 us (0.905)
  blocking collectives: 0 us -> 38.8 us
  waiting for transfers between devices: 57.7 us -> 33.9 us
  other arithmetic: 15.6 us -> 3.02 us
  starting transfers between devices: 38.6 us -> 26.7 us
  local copies, waits for them, and re-layouts: 22.9 us -> 18.6 us
    all_to_all x0 -> x1, blocking collectives: none -> 38.8 us  [body(): lax.all_to_all(my_features, 'ep', split_axis=0, concat_axis=0, tiled=True)]
    all_to_all x2 -> x0, starting transfers between devices: 22.4 us -> none  [the longest x1 18.4 us: body(): lax.all_to_all(my_features, 'ep', split_axis=0, concat_axis=0, tiled=True)]
    all_to_all x2 -> x0, waiting for transfers between devices: 14.2 us -> none  [the longest x1 8.05 us: body(): lax.all_to_all(down_matrix, 'tp', split_axis=2, concat_axis=1, tiled=True)]
    unnamed x1 -> x0, other arithmetic: 11.5 us -> none
    ppermute x0 -> x3, starting transfers between devices: none -> 10.9 us  [rotated_exchange(): lax.ppermute(sent, axis, [(i, (i + step) % peers) for i in range(peers)])]
    all_to_all x2, waiting for transfers between devices: 23.1 us -> 13.6 us  [sent_to_all(): return lax.all_to_all(copies, axis, split_axis=0, concat_axis=0, tiled=True)]
    unnamed x20, local copies, waits for them, and re-layouts: 4.89 us -> 1.35 us
  transfers between devices with their start and end apart: 5 -> 6, of which waited for: 5 -> 3; matrix products, arithmetic and copies ran while one was open for 12% -> 3% of each run, Pallas kernels for 0% -> 0%
where the time goes in v1:
time: 124 us; the launch traced here: 123 us
  blocking collectives  38.8 us (31%)
  waiting for transfers between devices  33.9 us (27%)
  starting transfers between devices  26.7 us (22%)
  local copies, waits for them, and re-layouts  18.6 us (15%)
  other arithmetic  3.02 us (2%)
  matrix products  1.81 us (1%)
    all_to_all x1, blocking collectives, body(): lax.all_to_all(my_features, 'ep', split_axis=0, concat_axis=0, tiled=True)  38.8 us
    all_to_all x1, waiting for transfers between devices, body(): lax.all_to_all(summed, 'ep', split_axis=0, concat_axis=0, tiled=True)  20.4 us
    all_to_all x2, waiting for transfers between devices, sent_to_all(): return lax.all_to_all(copies, axis, split_axis=0, concat_axis=0, tiled=True)  13.6 us
    ppermute x3, starting transfers between devices, rotated_exchange(): lax.ppermute(sent, axis, [(i, (i + step) % peers) for i in range(peers)])  10.9 us
    all_to_all x1, starting transfers between devices, body(): lax.all_to_all(summed, 'ep', split_axis=0, concat_axis=0, tiled=True)  8.17 us
    all_to_all x2, starting transfers between devices, sent_to_all(): return lax.all_to_all(copies, axis, split_axis=0, concat_axis=0, tiled=True)  7.59 us
    scatter x1, local copies, waits for them, and re-layouts, body(): jnp.zeros((experts * capacity, model_width), jnp.bfloat16).at[target]  5.92 us
  transfers between devices with their start and end apart: 6, of which 3 were waited for; matrix products, arithmetic and copies ran while one was open for 3% of the time, Pallas kernels for 0%

profile of v1, /device:TPU:1, one launch (start us, length us, event | category | flops | bytes accessed | tf_op | source)
XLA Modules:
  0.0 123.2 jit_solution(9351460658881410709)
XLA Ops:
  0.0 0.9 copy.34
  1.2 0.7 broadcast_multiply_fusion
  3.1 5.9 %scatter_custom_fusion = bf16[384,2048]{1,0:T(8,128)(2,1)S(1)} fusion(s32[256]{0:T(256)S(1)} %bitcast.92, bf16[128,2048]{1,0:T(8,128)(2,1)S(1)} %fusion.6, s32[1024]{0:T(1024)S(1)} %pad_clamp_fusion.1, bf16[]{:T(256)} %constant.73.clone.1), kind=kCustom, calls=%fused_computation.16 | custom fusion | bytes 1572866 | tf_op jit(solution)/shard_map/scatter | solution.py:90
  9.1 2.3 %reshape.201 = bf16[128,3,2048]{2,1,0:T(4,128)(2,1)} reshape(bf16[384,2048]{1,0:T(8,128)(2,1)S(1)} %scatter_custom_fusion) | data formatting | bytes 3145728 | tf_op jit(solution)/shard_map/reshape | solution.py:92
  11.4 1.2 constant_dynamic-slice_fusion
  12.6 38.8 %all_to_all.20 = bf16[128,3,512]{2,1,0:T(4,128)(2,1)S(1)} all-to-all(bf16[128,3,512]{2,1,0:T(4,128)(2,1)S(1)} %constant_dynamic-slice_fusion), channel_id=1, replica_groups=mesh['ep'=128,'tp'=4] {'ep'}, dimensions={0} | all-to-all | bytes 786432 | tf_op jit(solution)/shard_map/all_to_all | solution.py:97
  51.5 1.3 %broadcast_in_dim.7 = bf16[4,128,3,512]{3,1,2,0:T(8,128)(2,1)} broadcast(bf16[128,3,512]{2,0,1:T(8,128)(2,1)S(1)} %copy.38), dimensions={1,2,3} | broadcast | bytes 1966080 | tf_op jit(solution)/shard_map/broadcast_in_dim | solution.py:37
  52.8 4.1 %all-to-all-start.1 = ((bf16[4,128,3,512]{3,1,2,0:T(8,128)(2,1)}), bf16[4,128,3,512]{3,1,2,0:T(8,128)(2,1)S(1)}, u32[]{:S(2)}, u32[]{:S(2)}) async-start(bf16[4,128,3,512]{3,1,2,0:T(8,128)(2,1)} %broadcast_in_dim.7), calls=%async_computation.1 | async-start | bytes 3145728 | tf_op jit(solution)/shard_map/all_to_all | solution.py:38
  57.2 0.8 constant_dynamic-slice_fusion.4
  58.1 3.4 %collective-permute-start = (bf16[1,96,512]{2,1,0:T(8,128)(2,1)S(1)}, bf16[1,96,512]{2,1,0:T(8,128)(2,1)S(1)}, u32[]{:S(2)}, u32[]{:S(2)}) collective-permute-start(bf16[1,96,512]{2,1,0:T(8,128)(2,1)S(1)} %bitcast.87), channel_id=1, source_target_pairs={{0,1},{1,2},{2,3},{3,0},{4,5},{5,6},{6,7},{7,4},{8,9},{9,10},{10,1... | collective-permute-start | bytes 294920 | tf_op jit(solution)/shard_map/ppermute | solution.py:25
  61.5 4.3 %collective-permute-start.1 = (bf16[1,96,512]{2,1,0:T(8,128)(2,1)S(1)}, bf16[1,96,512]{2,1,0:T(8,128)(2,1)S(1)}, u32[]{:S(2)}, u32[]{:S(2)}) collective-permute-start(bf16[1,96,512]{2,1,0:T(8,128)(2,1)S(1)} %bitcast.88), channel_id=1, source_target_pairs={{0,2},{1,3},{2,0},{3,1},{4,6},{5,7},{6,4},{7,5},{8,10},{9,11},{10,... | collective-permute-start | bytes 294920 | tf_op jit(solution)/shard_map/ppermute | solution.py:25
  65.8 3.3 %collective-permute-start.2 = (bf16[1,96,512]{2,1,0:T(8,128)(2,1)S(1)}, bf16[1,96,512]{2,1,0:T(8,128)(2,1)S(1)}, u32[]{:S(2)}, u32[]{:S(2)}) collective-permute-start(bf16[1,96,512]{2,1,0:T(8,128)(2,1)S(1)} %bitcast.89), channel_id=1, source_target_pairs={{0,3},{1,0},{2,1},{3,2},{4,7},{5,4},{6,5},{7,6},{8,11},{9,8},{10,9... | collective-permute-start | bytes 294920 | tf_op jit(solution)/shard_map/ppermute | solution.py:25
  69.2 8.6 %all-to-all-done.1 = bf16[4,128,3,512]{3,1,2,0:T(8,128)(2,1)S(1)} async-done(((bf16[4,128,3,512]{3,1,2,0:T(8,128)(2,1)}), bf16[4,128,3,512]{3,1,2,0:T(8,128)(2,1)S(1)}, u32[]{:S(2)}, u32[]{:S(2)}) %all-to-all-start.1) | async-done | bytes 1572896 | tf_op jit(solution)/shard_map/all_to_all | solution.py:38
  78.0 0.6 convolution_bitcast_fusion.1
  79.0 0.6 fusion.3
  79.5 0.7 broadcast_in_dim.8
  80.3 3.5 %all-to-all-start.2 = ((bf16[4,128,3,96]{1,3,2,0:T(8,128)(2,1)}), bf16[4,128,3,96]{1,3,2,0:T(8,128)(2,1)S(1)}, u32[]{:S(2)}, u32[]{:S(2)}) async-start(bf16[4,128,3,96]{1,3,2,0:T(8,128)(2,1)} %broadcast_in_dim.8), calls=%async_computation.2 | async-start | bytes 589824 | tf_op jit(solution)/shard_map/all_to_all | solution.py:38
  84.5 5.0 %all-to-all-done.2 = bf16[4,128,3,96]{1,3,2,0:T(8,128)(2,1)S(1)} async-done(((bf16[4,128,3,96]{1,3,2,0:T(8,128)(2,1)}), bf16[4,128,3,96]{1,3,2,0:T(8,128)(2,1)S(1)}, u32[]{:S(2)}, u32[]{:S(2)}) %all-to-all-start.2) | async-done | bytes 294944 | tf_op jit(solution)/shard_map/all_to_all | solution.py:38
  89.4 0.6 fusion
  90.0 1.2 copy.40
  91.2 8.2 %all-to-all-start.3 = ((bf16[128,3,512]{2,1,0:T(4,128)(2,1)}), bf16[128,3,512]{2,1,0:T(4,128)(2,1)S(1)}, u32[]{:S(2)}, u32[]{:S(2)}) async-start(bf16[128,3,512]{2,1,0:T(4,128)(2,1)} %copy.40), calls=%async_computation.3 | async-start | bytes 1048576 | tf_op jit(solution)/shard_map/all_to_all | solution.py:102
  99.6 20.4 %all-to-all-done.3 = bf16[128,3,512]{2,1,0:T(4,128)(2,1)S(1)} async-done(((bf16[128,3,512]{2,1,0:T(4,128)(2,1)}), bf16[128,3,512]{2,1,0:T(4,128)(2,1)S(1)}, u32[]{:S(2)}, u32[]{:S(2)}) %all-to-all-start.3) | async-done | bytes 393248 | tf_op jit(solution)/shard_map/all_to_all | solution.py:102
  120.3 1.2 gather_fusion.1
  121.8 1.4 %multiply_reduce_fusion = bf16[128,512]{1,0:T(8,128)(2,1)} fusion(f32[128,2,512]{2,1,0:T(2,128)S(1)} %reshape.207, f32[128,2]{1,0:T(8,128)S(1)} %copy.41), kind=kLoop, calls=%fused_computation.19 | loop fusion | flops 196608 | bytes 656384 | tf_op jit(solution)/shard_map/reduce_sum | solution.py:106
  (53 shorter events, 4.0 us)
Async XLA Ops:
  0.0 78.0 %copy-start = (bf16[1,2048,96]{1,2,0:T(8,128)(2,1)S(1)}, bf16[1,2048,96]{1,2,0:T(8,128)(2,1)}, u32[]{:S(2)}) copy-start(bf16[1,2048,96]{1,2,0:T(8,128)(2,1)} %param.13) | copy-start | bytes 1179652
  0.0 2.7 %copy-start.1 = (bf16[128,2048]{1,0:T(8,128)(2,1)S(1)}, bf16[128,2048]{1,0:T(8,128)(2,1)}, u32[]{:S(2)}) copy-start(bf16[128,2048]{1,0:T(8,128)(2,1)} %param.8) | copy-start | bytes 1572868
  0.0 2.9 %copy-start.4 = (f32[2048]{0:T(1024)S(1)}, f32[2048]{0:T(1024)}, u32[]{:S(2)}) copy-start(f32[2048]{0:T(1024)} %param.9) | copy-start | bytes 24580
  52.8 4.1 %copy-start.2 = (bf16[1,96,2048]{2,1,0:T(8,128)(2,1)S(1)}, bf16[1,96,2048]{2,1,0:T(8,128)(2,1)}, u32[]{:S(2)}) copy-start(bf16[1,96,2048]{2,1,0:T(8,128)(2,1)} %param.15) | copy-start | bytes 1179652
  52.8 25.0 %all-to-all-start.1 = ((bf16[4,128,3,512]{3,1,2,0:T(8,128)(2,1)}), bf16[4,128,3,512]{3,1,2,0:T(8,128)(2,1)S(1)}, u32[]{:S(2)}, u32[]{:S(2)}) async-start(bf16[4,128,3,512]{3,1,2,0:T(8,128)(2,1)} %broadcast_in_dim.7), calls=%async_computation.1 | async-start | bytes 3145728 | tf_op jit(solution)/shard_map/all_to_all | solution.py:38
  58.1 25.7 %collective-permute-start = (bf16[1,96,512]{2,1,0:T(8,128)(2,1)S(1)}, bf16[1,96,512]{2,1,0:T(8,128)(2,1)S(1)}, u32[]{:S(2)}, u32[]{:S(2)}) collective-permute-start(bf16[1,96,512]{2,1,0:T(8,128)(2,1)S(1)} %bitcast.87), channel_id=1, source_target_pairs={{0,1},{1,2},{2,3},{3,0},{4,5},{5,6},{6,7},{7,4},{8,9},{9,10},{10,1... | collective-permute-start | bytes 294920 | tf_op jit(solution)/shard_map/ppermute | solution.py:25
  61.5 22.3 %collective-permute-start.1 = (bf16[1,96,512]{2,1,0:T(8,128)(2,1)S(1)}, bf16[1,96,512]{2,1,0:T(8,128)(2,1)S(1)}, u32[]{:S(2)}, u32[]{:S(2)}) collective-permute-start(bf16[1,96,512]{2,1,0:T(8,128)(2,1)S(1)} %bitcast.88), channel_id=1, source_target_pairs={{0,2},{1,3},{2,0},{3,1},{4,6},{5,7},{6,4},{7,5},{8,10},{9,11},{10,... | collective-permute-start | bytes 294920 | tf_op jit(solution)/shard_map/ppermute | solution.py:25
  65.8 18.0 %collective-permute-start.2 = (bf16[1,96,512]{2,1,0:T(8,128)(2,1)S(1)}, bf16[1,96,512]{2,1,0:T(8,128)(2,1)S(1)}, u32[]{:S(2)}, u32[]{:S(2)}) collective-permute-start(bf16[1,96,512]{2,1,0:T(8,128)(2,1)S(1)} %bitcast.89), channel_id=1, source_target_pairs={{0,3},{1,0},{2,1},{3,2},{4,7},{5,4},{6,5},{7,6},{8,11},{9,8},{10,9... | collective-permute-start | bytes 294920 | tf_op jit(solution)/shard_map/ppermute | solution.py:25
  77.9 1.0 copy-start.6
  80.3 9.1 %all-to-all-start.2 = ((bf16[4,128,3,96]{1,3,2,0:T(8,128)(2,1)}), bf16[4,128,3,96]{1,3,2,0:T(8,128)(2,1)S(1)}, u32[]{:S(2)}, u32[]{:S(2)}) async-start(bf16[4,128,3,96]{1,3,2,0:T(8,128)(2,1)} %broadcast_in_dim.8), calls=%async_computation.2 | async-start | bytes 589824 | tf_op jit(solution)/shard_map/all_to_all | solution.py:38
  84.4 15.0 %copy-start.3 = (f32[128,2]{0,1:T(2,128)S(1)}, f32[128,2]{0,1:T(2,128)}, u32[]{:S(2)}) copy-start(f32[128,2]{0,1:T(2,128)} %param.12) | copy-start | bytes 3076
  84.5 15.0 %copy-start.5 = (f32[128]{0:T(128)S(1)}, f32[128]{0:T(128)}, u32[]{:S(2)}) copy-start(f32[128]{0:T(128)} %param.11) | copy-start | bytes 1540
  91.2 28.7 %all-to-all-start.3 = ((bf16[128,3,512]{2,1,0:T(4,128)(2,1)}), bf16[128,3,512]{2,1,0:T(4,128)(2,1)S(1)}, u32[]{:S(2)}, u32[]{:S(2)}) async-start(bf16[128,3,512]{2,1,0:T(4,128)(2,1)} %copy.40), calls=%async_computation.3 | async-start | bytes 1048576 | tf_op jit(solution)/shard_map/all_to_all | solution.py:102
